TPU v7x, 32 devices: a whole 2x2x4 slice. The times are simulated.
32 devices in a mesh: sp: 8 (over z, x), tp: 4 (over y, core).
Axes of the slice: x: 2, y: 2, z: 4, core: 2. Of those that a mesh axis runs over, the one named last changes fastest.
Arguments:
- residual: bfloat16 [3072, 2048], P('sp', 'tp'), may hold values from -6 to 6
- query_nope: bfloat16 [3072, 4096], P('sp', 'tp'), may hold values from -9 to 9
- query_rope: bfloat16 [3072, 2048], P('sp', 'tp'), may hold values from -600 to 600
- latent: bfloat16 [3072, 512], P('sp'), may hold values from -6 to 6
- rope_key: bfloat16 [3072, 64], P('sp'), may hold values from -6 to 6
- doc_ids: int32 [3072], P('sp'), may hold values from 0 to 3, never falling along the last dimension, each value on 1 to 1152 neighbouring positions
- key_up: bfloat16 [512, 4096], P(None, 'tp'), may hold values from -0.25 to 0.25
- value_up: bfloat16 [512, 4096], P(None, 'tp'), may hold values from -0.25 to 0.25
- out_proj: bfloat16 [4096, 2048], P('tp'), may hold values from -0.375 to 0.375
- norm1_gain: bfloat16 [2048], P('tp'), may hold values from 0.099609375 to 1.8984375
- norm1_bias: bfloat16 [2048], P('tp'), may hold values from -3 to 3
- ffn_gate: bfloat16 [2048, 5632], P('sp', 'tp'), may hold values from -0.125 to 0.125
- ffn_value: bfloat16 [2048, 5632], P('sp', 'tp'), may hold values from -0.125 to 0.125
- conv_gate: bfloat16 [3, 5632], P(None, 'tp'), may hold values from -3.5 to 3.5
- conv_value: bfloat16 [3, 5632], P(None, 'tp'), may hold values from -3.5 to 3.5
- ffn_down: bfloat16 [5632, 2048], P('tp', 'sp'), may hold values from -0.15625 to 0.15625
- norm2_gain: bfloat16 [2048], P('tp'), may hold values from 0.099609375 to 1.8984375
- norm2_bias: bfloat16 [2048], P('tp'), may hold values from -3 to 3
Outputs:
- layer_out: bfloat16 [3072, 2048], P('sp', 'tp')
Inputs may be any that keep to these rules, and one draw needn't show every extreme that they name: `doc_ids`: document numbers never fall along the positions; each document holds 1 to 1152 positions, and one holds exactly 1152.
All inputs are finite; a program needn't handle non-finite values.
Results may differ from a plain program's by a relative error of at most 0.014.
Values may be sent and summed in bfloat16 or wider, within the bound.
A program may use at most 128 MiB of HBM per device.

v0:
```python
import jax
import jax.numpy as jnp
from jax import lax
from jax.sharding import PartitionSpec as P

D = 2048
NOPE = 128
ROPE = 64
VDIM = 128
CONV = 3
REACH = 3
norm_eps = 1e-05
residual_scale = 8.0**0.25
rope_base_freq = 10000.0
masked_score = -1e30


def passed_along(value, axis, by):
    count = lax.axis_size(axis)
    pairs = [(i, i + by) for i in range(count) if 0 <= i + by < count]
    return lax.ppermute(value, axis, pairs)


def tables(positions):
    frequencies = 1.0 / rope_base_freq ** (jnp.arange(0, ROPE, 2, dtype=jnp.float32) / ROPE)
    angles = positions.astype(jnp.float32)[:, None] * frequencies[None, :]
    return (jnp.cos(angles), jnp.sin(angles))


def rotate(vectors, cosine, sine_table):
    half_width = vectors.shape[-1] // 2
    front_half = vectors[..., :half_width]
    back_half = vectors[..., half_width:]
    return jnp.concatenate(
        [
            front_half * cosine - back_half * sine_table,
            front_half * sine_table + back_half * cosine,
        ],
        axis=-1,
    )


def scatter_sum(terms, axis):
    count = lax.axis_size(axis)
    width = terms.shape[1] // count
    parts = jnp.stack([terms[:, i * width : (i + 1) * width] for i in range(count)])
    got = lax.all_to_all(parts.astype(jnp.bfloat16), axis, 0, 0)
    return jnp.sum(got.astype(jnp.float32), 0)


def finish(mixed, totals, gain_row, bias_row):
    row_mean = totals[0][:, None] / D
    row_power = totals[1][:, None] / D
    return (mixed - row_mean) * lax.rsqrt(
        row_power - row_mean * row_mean + norm_eps
    ) * gain_row.astype(jnp.float32) + bias_row.astype(jnp.float32)


def local(
    residual,
    query_nope,
    query_rope,
    latent,
    rope_key,
    doc_ids,
    key_up,
    value_up,
    out_proj,
    norm1_gain,
    norm1_bias,
    ffn_gate,
    ffn_value,
    conv_gate,
    conv_value,
    ffn_down,
    norm2_gain,
    norm2_bias,
):
    row_count = latent.shape[0]
    head_count = query_nope.shape[1] // NOPE
    local_units = ffn_gate.shape[1]
    rim_rows = CONV - 1
    whole_gate, whole_value, whole_down = (
        lax.all_gather(ffn_gate, "sp", axis=0, tiled=True),
        lax.all_gather(ffn_value, "sp", axis=0, tiled=True),
        lax.all_gather(ffn_down, "sp", axis=1, tiled=True),
    )
    offset = lax.axis_index("sp") * row_count
    positions = offset + jnp.arange(row_count, dtype=jnp.int32)
    cosine, sine_table = tables(positions)
    turned_key = rotate(rope_key.astype(jnp.float32), cosine, sine_table).astype(jnp.bfloat16)
    turned_query = rotate(
        query_rope.astype(jnp.float32).reshape(row_count, head_count, ROPE),
        cosine[:, None],
        sine_table[:, None],
    ).astype(jnp.bfloat16)
    latent_list = []
    rim_list = []
    doc_list = []
    for shift_step in range(REACH, 0, -1):
        far_latent, far_key, far_doc = passed_along((latent, turned_key, doc_ids), "sp", shift_step)
        latent_list.append(far_latent)
        rim_list.append(far_key)
        doc_list.append(far_doc)
    win_latent = jnp.concatenate(latent_list + [latent], 0)
    win_key = jnp.concatenate(rim_list + [turned_key], 0)
    win_doc = jnp.concatenate(doc_list + [doc_ids], 0)
    key_rows = jnp.dot(win_latent, key_up, preferred_element_type=jnp.float32).astype(jnp.bfloat16)
    values = jnp.dot(win_latent, value_up, preferred_element_type=jnp.float32).astype(jnp.bfloat16)
    window = key_rows.shape[0]
    key_pos = offset - REACH * row_count + jnp.arange(window, dtype=jnp.int32)
    allowed = (
        (key_pos[None, :] <= positions[:, None])
        & (key_pos[None, :] >= 0)
        & (win_doc[None, :] == doc_ids[:, None])
    )
    scale = (NOPE + ROPE) ** (-0.5)
    scores = jnp.einsum(
        "qhd,khd->hqk",
        query_nope.reshape(row_count, head_count, NOPE),
        key_rows.reshape(window, head_count, NOPE),
        preferred_element_type=jnp.float32,
    )
    scores = scores + jnp.einsum(
        "qhr,kr->hqk", turned_query, win_key, preferred_element_type=jnp.float32
    )
    scores = jnp.where(allowed[None], scores * scale, masked_score)
    row_max = jnp.max(scores, -1, keepdims=True)
    weights = jnp.exp(scores - row_max)
    weights = (weights / jnp.sum(weights, -1, keepdims=True)).astype(jnp.bfloat16)
    attended = jnp.einsum(
        "hqk,khd->qhd",
        weights,
        values.reshape(window, head_count, VDIM),
        preferred_element_type=jnp.float32,
    )
    attended = attended.astype(jnp.bfloat16).reshape(row_count, head_count * VDIM)
    head_terms = jnp.dot(attended, out_proj, preferred_element_type=jnp.float32)
    projected = scatter_sum(head_terms, "tp")
    mixed_one = residual_scale * residual.astype(jnp.float32) + projected
    totals_one = lax.psum((jnp.sum(mixed_one, 1), jnp.sum(mixed_one * mixed_one, 1)), "tp")
    normed = finish(mixed_one, totals_one, norm1_gain, norm1_bias).astype(jnp.bfloat16)
    half = row_count // 2
    full_rows = jnp.concatenate(
        [
            lax.all_gather(normed[:half], "tp", axis=1, tiled=True),
            lax.all_gather(normed[half:], "tp", axis=1, tiled=True),
        ],
        0,
    )
    gate_sum = jnp.dot(full_rows, whole_gate, preferred_element_type=jnp.float32)
    value_sum = jnp.dot(full_rows, whole_value, preferred_element_type=jnp.float32)
    gate_pre = gate_sum.astype(jnp.bfloat16)
    value_pre = value_sum.astype(jnp.bfloat16)
    tail_gate, tail_value, tail_doc = passed_along(
        (
            gate_pre[row_count - rim_rows :],
            value_pre[row_count - rim_rows :],
            doc_ids[row_count - rim_rows :],
        ),
        "sp",
        1,
    )
    ext_gate = jnp.concatenate([tail_gate, gate_pre], 0)
    ext_value = jnp.concatenate([tail_value, value_pre], 0)
    ext_doc = jnp.concatenate([tail_doc, doc_ids], 0)
    gate_mix = jnp.zeros((row_count, local_units), jnp.float32)
    value_mix = jnp.zeros((row_count, local_units), jnp.float32)
    for tap_index in range(CONV):
        valid_tap = (
            (ext_doc[tap_index : tap_index + row_count] == doc_ids)
            & (positions - rim_rows + tap_index >= 0)
        ).astype(jnp.float32)[:, None]
        gate_mix = (
            gate_mix
            + conv_gate[tap_index].astype(jnp.float32)
            * ext_gate[tap_index : tap_index + row_count].astype(jnp.float32)
            * valid_tap
        )
        value_mix = (
            value_mix
            + conv_value[tap_index].astype(jnp.float32)
            * ext_value[tap_index : tap_index + row_count].astype(jnp.float32)
            * valid_tap
        )
    hidden = (value_mix * jax.nn.gelu(gate_mix)).astype(jnp.bfloat16)
    unit_terms = jnp.dot(hidden, whole_down, preferred_element_type=jnp.float32)
    ffn_out = scatter_sum(unit_terms, "tp")
    mixed_two = residual_scale * normed.astype(jnp.float32) + ffn_out
    totals_two = lax.psum((jnp.sum(mixed_two, 1), jnp.sum(mixed_two * mixed_two, 1)), "tp")
    return finish(mixed_two, totals_two, norm2_gain, norm2_bias).astype(jnp.bfloat16)


def solution(mesh):
    placed = (
        P("sp", "tp"),
        P("sp", "tp"),
        P("sp", "tp"),
        P("sp", None),
        P("sp", None),
        P("sp"),
        P(None, "tp"),
        P(None, "tp"),
        P("tp", None),
        P("tp"),
        P("tp"),
        P("sp", "tp"),
        P("sp", "tp"),
        P(None, "tp"),
        P(None, "tp"),
        P("tp", "sp"),
        P("tp"),
        P("tp"),
    )
    return jax.shard_map(
        local, mesh=mesh, in_specs=placed, out_specs=P("sp", "tp"), check_vma=False
    )
```

profile of v0, /device:TPU:0, one launch (start us, length us, event | category | flops | bytes accessed | tf_op | source)
XLA Modules:
  0.0 366.7 jit_solution(3545293043475565079)
XLA Ops:
  9.2 5.9 %collective-permute-start.6 = (bf16[384,64]{0,1:T(8,128)(2,1)S(1)}, bf16[384,64]{0,1:T(8,128)(2,1)S(1)}, u32[]{:S(2)}, u32[]{:S(2)}) collective-permute-start(bf16[384,64]{0,1:T(8,128)(2,1)S(1)} %pad_maximum_fusion.4), channel_id=1, source_target_pairs={{0,12},{4,16},{8,20},{12,24},{16,28},{1,13},{5,17},{9,21},{13,25},... | collective-permute-start | bytes 147464 | tf_op jit(solution)/shard_map/ppermute | solution.py:21
  15.1 3.5 collective-permute-start.7
  18.6 2.9 collective-permute-start.3
  23.4 2.8 collective-permute-start.5
  26.6 2.6 collective-permute-start
  30.5 3.4 collective-permute-start.2
  35.3 11.7 %collective-permute-done = bf16[384,512]{1,0:T(8,128)(2,1)S(1)} collective-permute-done((bf16[384,512]{1,0:T(8,128)(2,1)S(1)}, bf16[384,512]{1,0:T(8,128)(2,1)S(1)}, u32[]{:S(2)}, u32[]{:S(2)}) %collective-permute-start) | collective-permute-done | bytes 393248 | tf_op jit(solution)/shard_map/ppermute | solution.py:21
  47.1 3.3 collective-permute-start.8
  50.4 11.0 %collective-permute-done.1 = bf16[384,512]{1,0:T(8,128)(2,1)S(1)} collective-permute-done((bf16[384,512]{1,0:T(8,128)(2,1)S(1)}, bf16[384,512]{1,0:T(8,128)(2,1)S(1)}, u32[]{:S(2)}, u32[]{:S(2)}) %collective-permute-start.1) | collective-permute-done | bytes 393248 | tf_op jit(solution)/shard_map/ppermute | solution.py:21
  63.5 8.3 %fusion.30 = f32[8,1536,384]{2,1,0:T(8,128)} fusion(bf16[1536,8,128]{0,2,1:T(8,128)(2,1)S(1)} %bitcast.56, bf16[384,1024]{1,0:T(8,128)(2,1)S(1)} %copy-done.4), kind=kOutput, calls=%fused_computation.50 | convolution fusion | flops 1207959552 | bytes 22806528 | tf_op jit(solution)/shard_map/qhd,khd->hqk/dot_general | solution.py:118
  71.8 3.5 convolution_convert_fusion.1
  75.3 12.1 %fusion.2 = f32[8,384,1536]{1,2,0:T(8,128)} fusion(f32[8,1536,384]{2,1,0:T(8,128)} %fusion.30, pred[384,1536]{0,1:T(8,128)(4,1)S(1)} %compare_and_fusion, bf16[384,8,32]{0,2,1:T(8,128)(2,1)S(1)} %get-tuple-element.28, bf16[384,8,32]{0,2,1:T(8,128)(2,1)S(1)} %get-tuple-element.27, bf16[384,32]{0,1:T(8,128)(2,1)S(1)} %get-tuple-element.32, ...), kind=kOutput, calls=%fused_computation.3 | convolution fusion | flops 619905024 | bytes 38928384 | tf_op jit(solution)/shard_map/qhr,kr->hqk/dot_general | solution.py:124
  87.4 15.4 %fusion.61 = f32[8,384]{1,0:T(8,128)S(1)} fusion(f32[8,384,1536]{1,2,0:T(8,128)} %fusion.2), kind=kOutput, calls=%fused_computation.129 | output fusion | flops 9438719 | bytes 18886656 | tf_op jit(solution)/shard_map/sub | solution.py:129
  102.8 17.6 %fusion.13 = bf16[8,128,384]{2,1,0:T(8,128)(2,1)S(1)} fusion(bf16[1536,8,128]{0,2,1:T(8,128)(2,1)} %bitcast.57, f32[8,384]{1,0:T(8,128)S(1)} %fusion.61, f32[8,384,1536]{1,2,0:T(8,128)} %fusion.2), kind=kOutput, calls=%fused_computation.28 | convolution fusion | flops 1222513152 | bytes 22818816 | tf_op jit(solution)/shard_map/hqk,khd->qhd/dot_general | solution.py:131
  120.4 4.0 %convolution_convert_fusion.5 = bf16[384,2048]{1,0:T(8,128)(2,1)S(1)} fusion(bf16[384,1024]{0,1:T(8,128)(2,1)S(1)} %bitcast.58, bf16[1024,2048]{1,0:T(8,128)(2,1)} %param.26), kind=kOutput, calls=%fused_computation.15 | convolution fusion | flops 1611399168 | bytes 6553600 | tf_op jit(solution)/shard_map/dot_general | solution.py:138
  125.9 3.7 %all-to-all-start = ((bf16[4,384,512]{2,1,0:T(8,128)(2,1)}), bf16[4,384,512]{2,1,0:T(8,128)(2,1)S(1)}, u32[]{:S(2)}, u32[]{:S(2)}) async-start(bf16[4,384,512]{2,1,0:T(8,128)(2,1)} %pad_maximum_fusion), calls=%async_computation | async-start | bytes 3145728 | tf_op jit(solution)/shard_map/all_to_all | solution.py:47
  129.7 12.4 %collective-permute-start.10 = (s32[2]{0:T(128)S(1)}, s32[2]{0:T(128)S(1)}, u32[]{:S(2)}, u32[]{:S(2)}) collective-permute-start(s32[2]{0:T(128)S(1)} %slice.108), channel_id=1, source_target_pairs={{0,4},{4,8},{8,12},{12,16},{16,20},{20,24},{24,28},{1,5},{5,9},{9,... | collective-permute-start | bytes 32 | tf_op jit(solution)/shard_map/ppermute | solution.py:21
  143.5 6.1 %all-to-all-done = bf16[4,384,512]{2,1,0:T(8,128)(2,1)S(1)} async-done(((bf16[4,384,512]{2,1,0:T(8,128)(2,1)}), bf16[4,384,512]{2,1,0:T(8,128)(2,1)S(1)}, u32[]{:S(2)}, u32[]{:S(2)}) %all-to-all-start) | async-done | bytes 1572896 | tf_op jit(solution)/shard_map/all_to_all | solution.py:47
  150.2 6.1 %all-reduce.1 = (f32[384]{0:T(512)S(1)}, f32[384]{0:T(512)S(1)}) all-reduce(f32[384]{0:T(512)S(1)} %get-tuple-element.8, f32[384]{0:T(512)S(1)} %get-tuple-element.7), channel_id=1, replica_groups=mesh['sp'=8,'tp'=4] {'tp'}, use_global_device_ids=true, to_apply=%region_6.7 | all-reduce | flops 768 | bytes 6144 | tf_op jit(solution)/shard_map/psum | solution.py:141
  156.5 8.4 %all_gather.15 = bf16[192,2048]{1,0:T(8,128)(2,1)S(1)} all-gather(bf16[192,512]{1,0:T(8,128)(2,1)S(1)} %get-tuple-element.30), channel_id=1, replica_groups=mesh['sp'=8,'tp'=4] {'tp'}, dimensions={1}, use_global_device_ids=true | all-gather | bytes 983040 | tf_op jit(solution)/shard_map/all_gather | solution.py:146
  165.0 8.7 %all_gather.16 = bf16[192,2048]{1,0:T(8,128)(2,1)S(1)} all-gather(bf16[192,512]{1,0:T(8,128)(2,1)S(1)} %get-tuple-element.29), channel_id=1, replica_groups=mesh['sp'=8,'tp'=4] {'tp'}, dimensions={1}, use_global_device_ids=true | all-gather | bytes 983040 | tf_op jit(solution)/shard_map/all_gather | solution.py:147
  173.7 5.2 %convolution_convert_fusion.3 = bf16[384,1408]{1,0:T(8,128)(2,1)S(1)} fusion(bf16[384,2048]{1,0:T(8,128)(2,1)S(1)} %constant_dynamic-update-slice_fusion.4, bf16[2048,1408]{1,0:T(8,128)(2,1)} %all-gather.6.cloned.1.call-done), kind=kOutput, calls=%fused_computation.13 | convolution fusion | flops 2215133184 | bytes 8421376 | tf_op jit(solution)/shard_map/dot_general | solution.py:151
  180.0 12.5 %collective-permute-start.11 = (bf16[2,1408]{1,0:T(2,128)(2,1)S(1)}, bf16[2,1408]{1,0:T(2,128)(2,1)S(1)}, u32[]{:S(2)}, u32[]{:S(2)}) collective-permute-start(bf16[2,1408]{1,0:T(2,128)(2,1)S(1)} %slice.137), channel_id=1, source_target_pairs={{0,4},{4,8},{8,12},{12,16},{16,20},{20,24},{24,28},{1,5},{5,9},{9,... | collective-permute-start | bytes 16904 | tf_op jit(solution)/shard_map/ppermute | solution.py:21
  192.5 30.3 %all-gather.4.cloned.1.call-done = bf16[2048,1408]{1,0:T(8,128)(2,1)} async-done(((bf16[256,1408]{1,0:T(8,128)(2,1)}), bf16[2048,1408]{1,0:T(8,128)(2,1)}) %all-gather.4.cloned.1.call-update) | async-done | bytes 5767184 | tf_op jit(solution)/shard_map/all_gather | solution.py:85
  222.8 5.2 %convolution_convert_fusion.4 = bf16[384,1408]{1,0:T(8,128)(2,1)S(1)} fusion(bf16[384,2048]{1,0:T(8,128)(2,1)S(1)} %constant_dynamic-update-slice_fusion.4, bf16[2048,1408]{1,0:T(8,128)(2,1)} %all-gather.4.cloned.1.call-done), kind=kOutput, calls=%fused_computation.14 | convolution fusion | flops 2215133184 | bytes 8421376 | tf_op jit(solution)/shard_map/dot_general | solution.py:152
  228.1 2.5 collective-permute-start.9
  230.7 85.7 %all-gather.8.cloned.1.call-done = bf16[1408,2048]{1,0:T(8,128)(2,1)} async-done(((bf16[1408,256]{1,0:T(8,128)(2,1)}), bf16[1408,2048]{1,0:T(8,128)(2,1)}) %all-gather.8.cloned.1.call-update) | async-done | bytes 5767184 | tf_op jit(solution)/shard_map/all_gather | solution.py:86
  316.4 9.3 %convolution_convert_fusion.2 = bf16[384,2048]{1,0:T(8,128)(2,1)S(1)} fusion(bf16[1408,2048]{1,0:T(8,128)(2,1)} %all-gather.8.cloned.1.call-done, bf16[384,1408]{1,0:T(8,128)(2,1)} %copy-done.14, bf16[384,1408]{1,0:T(8,128)(2,1)} %copy-done.15, bf16[2,1408]{1,0:T(2,128)(2,1)S(1)} %collective-permute-done.11, ...), kind=kOutput, calls=%fused_computation.12 | convolution fusion | flops 2239168512 | bytes 9552384 | tf_op jit(solution)/shard_map/dot_general | solution.py:187
  327.2 3.7 %all-to-all-start.1 = ((bf16[4,384,512]{2,1,0:T(8,128)(2,1)}), bf16[4,384,512]{2,1,0:T(8,128)(2,1)S(1)}, u32[]{:S(2)}, u32[]{:S(2)}) async-start(bf16[4,384,512]{2,1,0:T(8,128)(2,1)} %pad_maximum_fusion.1), calls=%async_computation.1 | async-start | bytes 3145728 | tf_op jit(solution)/shard_map/all_to_all | solution.py:47
  331.0 20.0 %all-to-all-done.1 = bf16[4,384,512]{2,1,0:T(8,128)(2,1)S(1)} async-done(((bf16[4,384,512]{2,1,0:T(8,128)(2,1)}), bf16[4,384,512]{2,1,0:T(8,128)(2,1)S(1)}, u32[]{:S(2)}, u32[]{:S(2)}) %all-to-all-start.1) | async-done | bytes 1572896 | tf_op jit(solution)/shard_map/all_to_all | solution.py:47
  352.4 5.8 %all-reduce = (f32[384]{0:T(512)S(1)}, f32[384]{0:T(512)S(1)}) all-reduce(f32[384]{0:T(512)S(1)} %get-tuple-element.6, f32[384]{0:T(512)S(1)} %get-tuple-element.5), channel_id=1, replica_groups=mesh['sp'=8,'tp'=4] {'tp'}, use_global_device_ids=true, to_apply=%region_11.12 | all-reduce | flops 768 | bytes 6144 | tf_op jit(solution)/shard_map/psum | solution.py:190
  358.2 2.0 add_convert_fusion
  (95 shorter events, 17.3 us)
Async XLA Ops:
  6.5 55.0 %copy-start = (bf16[512,1024]{1,0:T(8,128)(2,1)S(1)}, bf16[512,1024]{1,0:T(8,128)(2,1)}, u32[]{:S(2)}) copy-start(bf16[512,1024]{1,0:T(8,128)(2,1)} %param.24) | copy-start | bytes 3145732
  6.5 19.7 %copy-start.6 = (bf16[384,512]{1,0:T(8,128)(2,1)S(1)}, bf16[384,512]{1,0:T(8,128)(2,1)}, u32[]{:S(2)}) copy-start(bf16[384,512]{1,0:T(8,128)(2,1)} %param.20) | copy-start | bytes 1179652
  6.5 167.2 %all-gather.6.cloned.1.call-start = ((), (), s32[]{:S(2)}) async-start(), calls=%async_computation.3 | async-start | bytes 6488064 | tf_op jit(solution)/shard_map/all_gather | solution.py:84
  7.3 19.3 %copy-start.5 = (bf16[384,512]{1,0:T(8,128)(2,1)S(1)}, bf16[384,512]{1,0:T(8,128)(2,1)}, u32[]{:S(2)}) copy-start(bf16[384,512]{1,0:T(8,128)(2,1)} %param.21) | copy-start | bytes 1179652
  7.3 26.6 %copy-start.7 = (s32[384]{0:T(512)S(1)}, s32[384]{0:T(512)}, u32[]{:S(2)}) copy-start(s32[384]{0:T(512)} %param.23) | copy-start | bytes 4612
  7.3 215.5 %all-gather.4.cloned.1.call-start = ((), (), s32[]{:S(2)}) async-start(), calls=%async_computation.2 | async-start | bytes 6488064 | tf_op jit(solution)/shard_map/all_gather | solution.py:85
  8.0 308.3 %all-gather.8.cloned.1.call-start = ((), (), s32[]{:S(2)}) async-start(), calls=%async_computation.4 | async-start | bytes 6488064 | tf_op jit(solution)/shard_map/all_gather | solution.py:86
  9.2 66.1 %collective-permute-start.6 = (bf16[384,64]{0,1:T(8,128)(2,1)S(1)}, bf16[384,64]{0,1:T(8,128)(2,1)S(1)}, u32[]{:S(2)}, u32[]{:S(2)}) collective-permute-start(bf16[384,64]{0,1:T(8,128)(2,1)S(1)} %pad_maximum_fusion.4), channel_id=1, source_target_pairs={{0,12},{4,16},{8,20},{12,24},{16,28},{1,13},{5,17},{9,21},{13,25},... | collective-permute-start | bytes 147464 | tf_op jit(solution)/shard_map/ppermute | solution.py:21
  15.1 60.2 %collective-permute-start.7 = (bf16[384,64]{0,1:T(8,128)(2,1)S(1)}, bf16[384,64]{0,1:T(8,128)(2,1)S(1)}, u32[]{:S(2)}, u32[]{:S(2)}) collective-permute-start(bf16[384,64]{0,1:T(8,128)(2,1)S(1)} %pad_maximum_fusion.4), channel_id=1, source_target_pairs={{0,8},{4,12},{8,16},{12,20},{16,24},{20,28},{1,9},{5,13},{9,17},{1... | collective-permute-start | bytes 147464 | tf_op jit(solution)/shard_map/ppermute | solution.py:21
  18.6 8.0 %collective-permute-start.3 = (s32[384]{0:T(512)}, s32[384]{0:T(512)S(1)}, u32[]{:S(2)}, u32[]{:S(2)}) collective-permute-start(s32[384]{0:T(512)} %param.23), channel_id=1, source_target_pairs={{0,12},{4,16},{8,20},{12,24},{16,28},{1,13},{5,17},{9,21},{13,25},... | collective-permute-start | bytes 4616 | tf_op jit(solution)/shard_map/ppermute | solution.py:21
  21.5 7.7 %collective-permute-start.4 = (s32[384]{0:T(512)}, s32[384]{0:T(512)S(1)}, u32[]{:S(2)}, u32[]{:S(2)}) collective-permute-start(s32[384]{0:T(512)} %param.23), channel_id=1, source_target_pairs={{0,8},{4,12},{8,16},{12,20},{16,24},{20,28},{1,9},{5,13},{9,17},{1... | collective-permute-start | bytes 4616 | tf_op jit(solution)/shard_map/ppermute | solution.py:21
  23.4 7.1 %collective-permute-start.5 = (s32[384]{0:T(512)}, s32[384]{0:T(512)S(1)}, u32[]{:S(2)}, u32[]{:S(2)}) collective-permute-start(s32[384]{0:T(512)} %param.23), channel_id=1, source_target_pairs={{0,4},{4,8},{8,12},{12,16},{16,20},{20,24},{24,28},{1,5},{5,9},{9,... | collective-permute-start | bytes 4616 | tf_op jit(solution)/shard_map/ppermute | solution.py:21
  26.6 20.5 %collective-permute-start = (bf16[384,512]{1,0:T(8,128)(2,1)S(1)}, bf16[384,512]{1,0:T(8,128)(2,1)S(1)}, u32[]{:S(2)}, u32[]{:S(2)}) collective-permute-start(bf16[384,512]{1,0:T(8,128)(2,1)S(1)} %copy-done.5), channel_id=1, source_target_pairs={{0,12},{4,16},{8,20},{12,24},{16,28},{1,13},{5,17},{9,21},{13,25},... | collective-permute-start | bytes 1179656 | tf_op jit(solution)/shard_map/ppermute | solution.py:21
  29.2 32.3 %collective-permute-start.1 = (bf16[384,512]{1,0:T(8,128)(2,1)S(1)}, bf16[384,512]{1,0:T(8,128)(2,1)S(1)}, u32[]{:S(2)}, u32[]{:S(2)}) collective-permute-start(bf16[384,512]{1,0:T(8,128)(2,1)S(1)} %copy-done.5), channel_id=1, source_target_pairs={{0,8},{4,12},{8,16},{12,20},{16,24},{20,28},{1,9},{5,13},{9,17},{1... | collective-permute-start | bytes 1179656 | tf_op jit(solution)/shard_map/ppermute | solution.py:21
  30.5 31.0 %collective-permute-start.2 = (bf16[384,512]{1,0:T(8,128)(2,1)S(1)}, bf16[384,512]{1,0:T(8,128)(2,1)S(1)}, u32[]{:S(2)}, u32[]{:S(2)}) collective-permute-start(bf16[384,512]{1,0:T(8,128)(2,1)S(1)} %copy-done.5), channel_id=1, source_target_pairs={{0,4},{4,8},{8,12},{12,16},{16,20},{20,24},{24,28},{1,5},{5,9},{9,... | collective-permute-start | bytes 1179656 | tf_op jit(solution)/shard_map/ppermute | solution.py:21
  47.1 28.3 %collective-permute-start.8 = (bf16[384,64]{0,1:T(8,128)(2,1)S(1)}, bf16[384,64]{0,1:T(8,128)(2,1)S(1)}, u32[]{:S(2)}, u32[]{:S(2)}) collective-permute-start(bf16[384,64]{0,1:T(8,128)(2,1)S(1)} %pad_maximum_fusion.4), channel_id=1, source_target_pairs={{0,4},{4,8},{8,12},{12,16},{16,20},{20,24},{24,28},{1,5},{5,9},{9,... | collective-permute-start | bytes 147464 | tf_op jit(solution)/shard_map/ppermute | solution.py:21
  63.5 8.3 %copy-start.16 = (bf16[512,1024]{1,0:T(8,128)(2,1)S(1)}, bf16[512,1024]{1,0:T(8,128)(2,1)}, u32[]{:S(2)}) copy-start(bf16[512,1024]{1,0:T(8,128)(2,1)} %param.25) | copy-start | bytes 3145732
  125.9 16.3 %copy-start.10 = (bf16[512]{0:T(512)(128)(2,1)S(1)}, bf16[512]{0:T(512)(128)(2,1)}, u32[]{:S(2)}) copy-start(bf16[512]{0:T(512)(128)(2,1)} %param.27) | copy-start | bytes 3076
  125.9 16.3 %copy-start.11 = (bf16[512]{0:T(512)(128)(2,1)S(1)}, bf16[512]{0:T(512)(128)(2,1)}, u32[]{:S(2)}) copy-start(bf16[512]{0:T(512)(128)(2,1)} %param.28) | copy-start | bytes 3076
  125.9 16.3 %copy-start.8 = (bf16[3,1408]{1,0:T(4,128)(2,1)S(1)}, bf16[3,1408]{1,0:T(4,128)(2,1)}, u32[]{:S(2)}) copy-start(bf16[3,1408]{1,0:T(4,128)(2,1)} %param.31) | copy-start | bytes 25348
  125.9 16.3 %copy-start.9 = (bf16[3,1408]{1,0:T(4,128)(2,1)S(1)}, bf16[3,1408]{1,0:T(4,128)(2,1)}, u32[]{:S(2)}) copy-start(bf16[3,1408]{1,0:T(4,128)(2,1)} %param.32) | copy-start | bytes 25348
  125.9 24.0 %copy-start.3 = (bf16[384,512]{1,0:T(8,128)(2,1)S(1)}, bf16[384,512]{1,0:T(8,128)(2,1)}, u32[]{:S(2)}) copy-start(bf16[384,512]{1,0:T(8,128)(2,1)} %param.18) | copy-start | bytes 1179652
  125.9 23.7 %all-to-all-start = ((bf16[4,384,512]{2,1,0:T(8,128)(2,1)}), bf16[4,384,512]{2,1,0:T(8,128)(2,1)S(1)}, u32[]{:S(2)}, u32[]{:S(2)}) async-start(bf16[4,384,512]{2,1,0:T(8,128)(2,1)} %pad_maximum_fusion), calls=%async_computation | async-start | bytes 3145728 | tf_op jit(solution)/shard_map/all_to_all | solution.py:47
  129.7 13.7 %collective-permute-start.10 = (s32[2]{0:T(128)S(1)}, s32[2]{0:T(128)S(1)}, u32[]{:S(2)}, u32[]{:S(2)}) collective-permute-start(s32[2]{0:T(128)S(1)} %slice.108), channel_id=1, source_target_pairs={{0,4},{4,8},{8,12},{12,16},{16,20},{20,24},{24,28},{1,5},{5,9},{9,... | collective-permute-start | bytes 32 | tf_op jit(solution)/shard_map/ppermute | solution.py:21
  156.5 17.2 %copy-start.2 = (bf16[384,512]{1,0:T(8,128)(2,1)}, bf16[384,512]{1,0:T(8,128)(2,1)S(1)}, u32[]{:S(2)}) copy-start(bf16[384,512]{1,0:T(8,128)(2,1)S(1)} %add_convert_fusion.1) | copy-start | bytes 1179652
  180.0 136.4 %collective-permute-start.11 = (bf16[2,1408]{1,0:T(2,128)(2,1)S(1)}, bf16[2,1408]{1,0:T(2,128)(2,1)S(1)}, u32[]{:S(2)}, u32[]{:S(2)}) collective-permute-start(bf16[2,1408]{1,0:T(2,128)(2,1)S(1)} %slice.137), channel_id=1, source_target_pairs={{0,4},{4,8},{8,12},{12,16},{16,20},{20,24},{24,28},{1,5},{5,9},{9,... | collective-permute-start | bytes 16904 | tf_op jit(solution)/shard_map/ppermute | solution.py:21
  228.0 2.5 copy-start.15
  228.1 88.3 %collective-permute-start.9 = (bf16[2,1408]{1,0:T(2,128)(2,1)S(1)}, bf16[2,1408]{1,0:T(2,128)(2,1)S(1)}, u32[]{:S(2)}, u32[]{:S(2)}) collective-permute-start(bf16[2,1408]{1,0:T(2,128)(2,1)S(1)} %slice.134), channel_id=1, source_target_pairs={{0,4},{4,8},{8,12},{12,16},{16,20},{20,24},{24,28},{1,5},{5,9},{9,... | collective-permute-start | bytes 16904 | tf_op jit(solution)/shard_map/ppermute | solution.py:21
  327.2 3.7 %copy-start.12 = (bf16[512]{0:T(512)(128)(2,1)S(1)}, bf16[512]{0:T(512)(128)(2,1)}, u32[]{:S(2)}) copy-start(bf16[512]{0:T(512)(128)(2,1)} %param.34) | copy-start | bytes 3076
  327.2 3.7 %copy-start.13 = (bf16[512]{0:T(512)(128)(2,1)S(1)}, bf16[512]{0:T(512)(128)(2,1)}, u32[]{:S(2)}) copy-start(bf16[512]{0:T(512)(128)(2,1)} %param.35) | copy-start | bytes 3076
  327.2 23.7 %all-to-all-start.1 = ((bf16[4,384,512]{2,1,0:T(8,128)(2,1)}), bf16[4,384,512]{2,1,0:T(8,128)(2,1)S(1)}, u32[]{:S(2)}, u32[]{:S(2)}) async-start(bf16[4,384,512]{2,1,0:T(8,128)(2,1)} %pad_maximum_fusion.1), calls=%async_computation.1 | async-start | bytes 3145728 | tf_op jit(solution)/shard_map/all_to_all | solution.py:47
  330.9 29.2 %copy-start.1 = (bf16[512,1024]{1,0:T(8,128)(2,1)S(1)}, bf16[512,1024]{1,0:T(8,128)(2,1)}, u32[]{:S(2)}) copy-start(bf16[512,1024]{1,0:T(8,128)(2,1)} %param.24) | copy-start | bytes 3145732
  (2 other events, 2.9 us)
Sparse Core Ops, SparseCore 0:
  9.5 118.1 all-gather.5
  129.9 92.8 all-gather.3
  224.8 91.4 all-gather.7
where the time goes:
time: 368 us; the launch traced here: 367 us
  waiting for transfers between devices  167 us (45%)
  matrix products  67.2 us (18%)
  starting transfers between devices  62.4 us (17%)
  blocking collectives  28.9 us (8%)
  other arithmetic  25.2 us (7%)
  between operations  13.7 us (4%)
    all_gather x1, waiting for transfers between devices, local(): lax.all_gather(ffn_down, 'sp', axis=1, tiled=True)  85.7 us
    ppermute x12, starting transfers between devices, passed_along(): return lax.ppermute(value, axis, pairs)  55 us
    all_gather x1, waiting for transfers between devices, local(): lax.all_gather(ffn_value, 'sp', axis=0, tiled=True)  30.3 us
    all_to_all x2, waiting for transfers between devices, scatter_sum(): got = lax.all_to_all(parts.astype(jnp.bfloat16), axis, 0, 0)  26.1 us
    ppermute x12, waiting for transfers between devices, passed_along(): return lax.ppermute(value, axis, pairs)  23.9 us
    dot_general x1, matrix products, local(): jnp.einsum('hqk,khd->qhd', weights, values.reshape(window, head_count, VD...  17.6 us
    sub x1, other arithmetic, local(): weights = jnp.exp(scores - row_max)  15.4 us
    dot_general x1, matrix products, local(): jnp.einsum('qhr,kr->hqk', turned_query, win_key, preferred_element_type=j...  12.1 us
  transfers between devices with their start and end apart: 17, of which 7 were waited for; matrix products, arithmetic and copies ran while one was open for 22% of the time, Pallas kernels for 0%

commit v1 on v0

--- a/solution.py
+++ b/solution.py
@@ -83,7 +83,7 @@
     whole_gate, whole_value, whole_down = (
         lax.all_gather(ffn_gate, "sp", axis=0, tiled=True),
         lax.all_gather(ffn_value, "sp", axis=0, tiled=True),
-        lax.all_gather(ffn_down, "sp", axis=1, tiled=True),
+        jnp.concatenate(lax.all_gather(ffn_down, "sp"), axis=1),
     )
     offset = lax.axis_index("sp") * row_count
     positions = offset + jnp.arange(row_count, dtype=jnp.int32)

time: 368 us -> 375 us (1.019)
  local copies, waits for them, and re-layouts: 1.76 us -> 10.1 us
    reshape x0 -> x1, local copies, waits for them, and re-layouts: none -> 8.34 us  [local(): jnp.concatenate(lax.all_gather(ffn_down, 'sp'), axis=1)]
  transfers between devices with their start and end apart: 17 -> 17, of which waited for: 7 -> 7; matrix products, arithmetic and copies ran while one was open for 22% -> 23% of each run, Pallas kernels for 0% -> 0%
where the time goes in v1:
time: 375 us; the launch traced here: 374 us
  waiting for transfers between devices  167 us (45%)
  matrix products  67.3 us (18%)
  starting transfers between devices  62.4 us (17%)
  blocking collectives  28.9 us (8%)
  other arithmetic  25.1 us (7%)
  between operations  13.7 us (4%)
  local copies, waits for them, and re-layouts  10.1 us (3%)
    all_gather x1, waiting for transfers between devices, local(): lax.all_gather(ffn_down, 'sp')  85 us
    ppermute x12, starting transfers between devices, passed_along(): return lax.ppermute(value, axis, pairs)  54.9 us
    all_gather x1, waiting for transfers between devices, local(): lax.all_gather(ffn_value, 'sp', axis=0, tiled=True)  30.4 us
    all_to_all x2, waiting for transfers between devices, scatter_sum(): got = lax.all_to_all(parts.astype(jnp.bfloat16), axis, 0, 0)  26.1 us
    ppermute x12, waiting for transfers between devices, passed_along(): return lax.ppermute(value, axis, pairs)  23.9 us
    dot_general x1, matrix products, local(): jnp.einsum('hqk,khd->qhd', weights, values.reshape(window, head_count, VD...  17.6 us
    sub x1, other arithmetic, local(): weights = jnp.exp(scores - row_max)  15.3 us
    dot_general x1, matrix products, local(): jnp.einsum('qhr,kr->hqk', turned_query, win_key, preferred_element_type=j...  12.1 us
  transfers between devices with their start and end apart: 17, of which 7 were waited for; matrix products, arithmetic and copies ran while one was open for 23% of the time, Pallas kernels for 0%

profile of v1, /device:TPU:0, one launch (start us, length us, event | category | flops | bytes accessed | tf_op | source)
XLA Modules:
  0.0 374.5 jit_solution(16778433980352434974)
XLA Ops:
  9.2 5.9 %collective-permute-start.6 = (bf16[384,64]{0,1:T(8,128)(2,1)S(1)}, bf16[384,64]{0,1:T(8,128)(2,1)S(1)}, u32[]{:S(2)}, u32[]{:S(2)}) collective-permute-start(bf16[384,64]{0,1:T(8,128)(2,1)S(1)} %pad_maximum_fusion.4), channel_id=1, source_target_pairs={{0,12},{4,16},{8,20},{12,24},{16,28},{1,13},{5,17},{9,21},{13,25},... | collective-permute-start | bytes 147464 | tf_op jit(solution)/shard_map/ppermute | solution.py:21
  15.1 3.5 collective-permute-start.7
  18.6 2.9 collective-permute-start.3
  23.4 2.8 collective-permute-start.5
  26.6 2.6 collective-permute-start
  30.5 3.4 collective-permute-start.2
  35.3 11.7 %collective-permute-done = bf16[384,512]{1,0:T(8,128)(2,1)S(1)} collective-permute-done((bf16[384,512]{1,0:T(8,128)(2,1)S(1)}, bf16[384,512]{1,0:T(8,128)(2,1)S(1)}, u32[]{:S(2)}, u32[]{:S(2)}) %collective-permute-start) | collective-permute-done | bytes 393248 | tf_op jit(solution)/shard_map/ppermute | solution.py:21
  47.1 3.3 collective-permute-start.8
  50.4 11.0 %collective-permute-done.1 = bf16[384,512]{1,0:T(8,128)(2,1)S(1)} collective-permute-done((bf16[384,512]{1,0:T(8,128)(2,1)S(1)}, bf16[384,512]{1,0:T(8,128)(2,1)S(1)}, u32[]{:S(2)}, u32[]{:S(2)}) %collective-permute-start.1) | collective-permute-done | bytes 393248 | tf_op jit(solution)/shard_map/ppermute | solution.py:21
  63.5 8.3 %fusion.30 = f32[8,1536,384]{2,1,0:T(8,128)} fusion(bf16[1536,8,128]{0,2,1:T(8,128)(2,1)S(1)} %bitcast.62, bf16[384,1024]{1,0:T(8,128)(2,1)S(1)} %copy-done.4), kind=kOutput, calls=%fused_computation.50 | convolution fusion | flops 1207959552 | bytes 22806528 | tf_op jit(solution)/shard_map/qhd,khd->hqk/dot_general | solution.py:118
  71.8 3.5 convolution_convert_fusion.1
  75.3 12.1 %fusion.2 = f32[8,384,1536]{1,2,0:T(8,128)} fusion(f32[8,1536,384]{2,1,0:T(8,128)} %fusion.30, pred[384,1536]{0,1:T(8,128)(4,1)S(1)} %compare_and_fusion, bf16[384,8,32]{0,2,1:T(8,128)(2,1)S(1)} %get-tuple-element.28, bf16[384,8,32]{0,2,1:T(8,128)(2,1)S(1)} %get-tuple-element.27, bf16[384,32]{0,1:T(8,128)(2,1)S(1)} %get-tuple-element.32, ...), kind=kOutput, calls=%fused_computation.3 | convolution fusion | flops 619905024 | bytes 38928384 | tf_op jit(solution)/shard_map/qhr,kr->hqk/dot_general | solution.py:124
  87.4 15.3 %fusion.61 = f32[8,384]{1,0:T(8,128)S(1)} fusion(f32[8,384,1536]{1,2,0:T(8,128)} %fusion.2), kind=kOutput, calls=%fused_computation.129 | output fusion | flops 9438719 | bytes 18886656 | tf_op jit(solution)/shard_map/sub | solution.py:129
  102.8 17.6 %fusion.13 = bf16[8,128,384]{2,1,0:T(8,128)(2,1)S(1)} fusion(bf16[1536,8,128]{0,2,1:T(8,128)(2,1)} %bitcast.63, f32[8,384]{1,0:T(8,128)S(1)} %fusion.61, f32[8,384,1536]{1,2,0:T(8,128)} %fusion.2), kind=kOutput, calls=%fused_computation.28 | convolution fusion | flops 1222513152 | bytes 22818816 | tf_op jit(solution)/shard_map/hqk,khd->qhd/dot_general | solution.py:131
  120.4 4.0 %convolution_convert_fusion.5 = bf16[384,2048]{1,0:T(8,128)(2,1)S(1)} fusion(bf16[384,1024]{0,1:T(8,128)(2,1)S(1)} %bitcast.64, bf16[1024,2048]{1,0:T(8,128)(2,1)} %param.26), kind=kOutput, calls=%fused_computation.15 | convolution fusion | flops 1611399168 | bytes 6553600 | tf_op jit(solution)/shard_map/dot_general | solution.py:138
  125.9 3.7 all-to-all-start
  129.7 12.4 %collective-permute-start.10 = (s32[2]{0:T(128)S(1)}, s32[2]{0:T(128)S(1)}, u32[]{:S(2)}, u32[]{:S(2)}) collective-permute-start(s32[2]{0:T(128)S(1)} %slice.108), channel_id=1, source_target_pairs={{0,4},{4,8},{8,12},{12,16},{16,20},{20,24},{24,28},{1,5},{5,9},{9,... | collective-permute-start | bytes 32 | tf_op jit(solution)/shard_map/ppermute | solution.py:21
  143.5 6.1 %all-to-all-done = bf16[4,384,512]{2,1,0:T(8,128)(2,1)S(1)} async-done(((bf16[4,384,512]{2,1,0:T(8,128)(2,1)}), bf16[4,384,512]{2,1,0:T(8,128)(2,1)S(1)}, u32[]{:S(2)}, u32[]{:S(2)}) %all-to-all-start) | async-done | bytes 1572896 | tf_op jit(solution)/shard_map/all_to_all | solution.py:47
  150.1 6.1 %all-reduce.1 = (f32[384]{0:T(512)S(1)}, f32[384]{0:T(512)S(1)}) all-reduce(f32[384]{0:T(512)S(1)} %get-tuple-element.8, f32[384]{0:T(512)S(1)} %get-tuple-element.7), channel_id=1, replica_groups=mesh['sp'=8,'tp'=4] {'tp'}, use_global_device_ids=true, to_apply=%region_6.7 | all-reduce | flops 768 | bytes 6144 | tf_op jit(solution)/shard_map/psum | solution.py:141
  156.5 8.4 %all_gather.18 = bf16[192,2048]{1,0:T(8,128)(2,1)S(1)} all-gather(bf16[192,512]{1,0:T(8,128)(2,1)S(1)} %get-tuple-element.30), channel_id=1, replica_groups=mesh['sp'=8,'tp'=4] {'tp'}, dimensions={1}, use_global_device_ids=true | all-gather | bytes 983040 | tf_op jit(solution)/shard_map/all_gather | solution.py:146
  164.9 8.7 %all_gather.19 = bf16[192,2048]{1,0:T(8,128)(2,1)S(1)} all-gather(bf16[192,512]{1,0:T(8,128)(2,1)S(1)} %get-tuple-element.29), channel_id=1, replica_groups=mesh['sp'=8,'tp'=4] {'tp'}, dimensions={1}, use_global_device_ids=true | all-gather | bytes 983040 | tf_op jit(solution)/shard_map/all_gather | solution.py:147
  173.7 5.2 %convolution_convert_fusion.3 = bf16[384,1408]{1,0:T(8,128)(2,1)S(1)} fusion(bf16[384,2048]{1,0:T(8,128)(2,1)S(1)} %constant_dynamic-update-slice_fusion.4, bf16[2048,1408]{1,0:T(8,128)(2,1)} %all-gather.7.cloned.1.call-done), kind=kOutput, calls=%fused_computation.13 | convolution fusion | flops 2215133184 | bytes 8421376 | tf_op jit(solution)/shard_map/dot_general | solution.py:151
  180.0 12.5 %collective-permute-start.11 = (bf16[2,1408]{1,0:T(2,128)(2,1)S(1)}, bf16[2,1408]{1,0:T(2,128)(2,1)S(1)}, u32[]{:S(2)}, u32[]{:S(2)}) collective-permute-start(bf16[2,1408]{1,0:T(2,128)(2,1)S(1)} %slice.137), channel_id=1, source_target_pairs={{0,4},{4,8},{8,12},{12,16},{16,20},{20,24},{24,28},{1,5},{5,9},{9,... | collective-permute-start | bytes 16904 | tf_op jit(solution)/shard_map/ppermute | solution.py:21
  192.4 30.4 %all-gather.5.cloned.1.call-done = bf16[2048,1408]{1,0:T(8,128)(2,1)} async-done(((bf16[256,1408]{1,0:T(8,128)(2,1)}), bf16[2048,1408]{1,0:T(8,128)(2,1)}) %all-gather.5.cloned.1.call-update) | async-done | bytes 5767184 | tf_op jit(solution)/shard_map/all_gather | solution.py:85
  222.8 5.2 %convolution_convert_fusion.4 = bf16[384,1408]{1,0:T(8,128)(2,1)S(1)} fusion(bf16[384,2048]{1,0:T(8,128)(2,1)S(1)} %constant_dynamic-update-slice_fusion.4, bf16[2048,1408]{1,0:T(8,128)(2,1)} %all-gather.5.cloned.1.call-done), kind=kOutput, calls=%fused_computation.14 | convolution fusion | flops 2215133184 | bytes 8421376 | tf_op jit(solution)/shard_map/dot_general | solution.py:152
  228.1 2.5 collective-permute-start.9
  230.7 85.0 %all-gather.9.cloned.1.call-done = bf16[11264,256]{1,0:T(8,128)(2,1)} async-done(((bf16[1408,256]{1,0:T(8,128)(2,1)}), bf16[11264,256]{1,0:T(8,128)(2,1)}) %all-gather.9.cloned.1.call-update) | async-done | bytes 5767184 | tf_op jit(solution)/shard_map/all_gather | solution.py:86
  315.7 8.3 %copy.31 = bf16[1408,8,256]{0,2,1:T(8,128)(2,1)} copy(bf16[1408,8,256]{2,0,1:T(8,128)(2,1)} %bitcast.59) | data formatting | bytes 11534336 | tf_op jit(solution)/shard_map/reshape | solution.py:86
  324.0 9.5 %convolution_convert_fusion.2 = bf16[384,2048]{1,0:T(8,128)(2,1)S(1)} fusion(bf16[1408,2048]{0,1:T(8,128)(2,1)} %bitcast.60, bf16[384,1408]{1,0:T(8,128)(2,1)S(1)} %copy-done.15, bf16[384,1408]{1,0:T(8,128)(2,1)} %copy-done.16, bf16[2,1408]{1,0:T(2,128)(2,1)S(1)} %collective-permute-done.11, bf16[2,1408]{1,0:T(2,128)(2,1)S(1)} %collective-permute-done.9, ...), kind=kOutput, calls=%fused_computation.12 | convolution fusion | flops 2239168512 | bytes 9552384 | tf_op jit(solution)/shard_map/dot_general | solution.py:187
  335.0 3.7 all-to-all-start.1
  338.7 20.0 %all-to-all-done.1 = bf16[4,384,512]{2,1,0:T(8,128)(2,1)S(1)} async-done(((bf16[4,384,512]{2,1,0:T(8,128)(2,1)}), bf16[4,384,512]{2,1,0:T(8,128)(2,1)S(1)}, u32[]{:S(2)}, u32[]{:S(2)}) %all-to-all-start.1) | async-done | bytes 1572896 | tf_op jit(solution)/shard_map/all_to_all | solution.py:47
  360.2 5.8 %all-reduce = (f32[384]{0:T(512)S(1)}, f32[384]{0:T(512)S(1)}) all-reduce(f32[384]{0:T(512)S(1)} %get-tuple-element.6, f32[384]{0:T(512)S(1)} %get-tuple-element.5), channel_id=1, replica_groups=mesh['sp'=8,'tp'=4] {'tp'}, use_global_device_ids=true, to_apply=%region_11.12 | all-reduce | flops 768 | bytes 6144 | tf_op jit(solution)/shard_map/psum | solution.py:190
  (98 shorter events, 19.3 us)
Async XLA Ops:
  6.5 55.0 %copy-start = (bf16[512,1024]{1,0:T(8,128)(2,1)S(1)}, bf16[512,1024]{1,0:T(8,128)(2,1)}, u32[]{:S(2)}) copy-start(bf16[512,1024]{1,0:T(8,128)(2,1)} %param.24) | copy-start | bytes 3145732
  6.5 19.7 %copy-start.6 = (bf16[384,512]{1,0:T(8,128)(2,1)S(1)}, bf16[384,512]{1,0:T(8,128)(2,1)}, u32[]{:S(2)}) copy-start(bf16[384,512]{1,0:T(8,128)(2,1)} %param.20) | copy-start | bytes 1179652
  6.5 167.1 %all-gather.7.cloned.1.call-start = ((), (), s32[]{:S(2)}) async-start(), calls=%async_computation.3 | async-start | bytes 6488064 | tf_op jit(solution)/shard_map/all_gather | solution.py:84
  7.3 19.3 %copy-start.5 = (bf16[384,512]{1,0:T(8,128)(2,1)S(1)}, bf16[384,512]{1,0:T(8,128)(2,1)}, u32[]{:S(2)}) copy-start(bf16[384,512]{1,0:T(8,128)(2,1)} %param.21) | copy-start | bytes 1179652
  7.3 26.6 %copy-start.7 = (s32[384]{0:T(512)S(1)}, s32[384]{0:T(512)}, u32[]{:S(2)}) copy-start(s32[384]{0:T(512)} %param.23) | copy-start | bytes 4612
  7.3 215.5 %all-gather.5.cloned.1.call-start = ((), (), s32[]{:S(2)}) async-start(), calls=%async_computation.2 | async-start | bytes 6488064 | tf_op jit(solution)/shard_map/all_gather | solution.py:85
  8.0 307.6 %all-gather.9.cloned.1.call-start = ((), (), s32[]{:S(2)}) async-start(), calls=%async_computation.4 | async-start | bytes 6488064 | tf_op jit(solution)/shard_map/all_gather | solution.py:86
  9.2 66.1 %collective-permute-start.6 = (bf16[384,64]{0,1:T(8,128)(2,1)S(1)}, bf16[384,64]{0,1:T(8,128)(2,1)S(1)}, u32[]{:S(2)}, u32[]{:S(2)}) collective-permute-start(bf16[384,64]{0,1:T(8,128)(2,1)S(1)} %pad_maximum_fusion.4), channel_id=1, source_target_pairs={{0,12},{4,16},{8,20},{12,24},{16,28},{1,13},{5,17},{9,21},{13,25},... | collective-permute-start | bytes 147464 | tf_op jit(solution)/shard_map/ppermute | solution.py:21
  15.1 60.2 %collective-permute-start.7 = (bf16[384,64]{0,1:T(8,128)(2,1)S(1)}, bf16[384,64]{0,1:T(8,128)(2,1)S(1)}, u32[]{:S(2)}, u32[]{:S(2)}) collective-permute-start(bf16[384,64]{0,1:T(8,128)(2,1)S(1)} %pad_maximum_fusion.4), channel_id=1, source_target_pairs={{0,8},{4,12},{8,16},{12,20},{16,24},{20,28},{1,9},{5,13},{9,17},{1... | collective-permute-start | bytes 147464 | tf_op jit(solution)/shard_map/ppermute | solution.py:21
  18.6 8.0 %collective-permute-start.3 = (s32[384]{0:T(512)}, s32[384]{0:T(512)S(1)}, u32[]{:S(2)}, u32[]{:S(2)}) collective-permute-start(s32[384]{0:T(512)} %param.23), channel_id=1, source_target_pairs={{0,12},{4,16},{8,20},{12,24},{16,28},{1,13},{5,17},{9,21},{13,25},... | collective-permute-start | bytes 4616 | tf_op jit(solution)/shard_map/ppermute | solution.py:21
  21.5 7.7 %collective-permute-start.4 = (s32[384]{0:T(512)}, s32[384]{0:T(512)S(1)}, u32[]{:S(2)}, u32[]{:S(2)}) collective-permute-start(s32[384]{0:T(512)} %param.23), channel_id=1, source_target_pairs={{0,8},{4,12},{8,16},{12,20},{16,24},{20,28},{1,9},{5,13},{9,17},{1... | collective-permute-start | bytes 4616 | tf_op jit(solution)/shard_map/ppermute | solution.py:21
  23.4 7.1 %collective-permute-start.5 = (s32[384]{0:T(512)}, s32[384]{0:T(512)S(1)}, u32[]{:S(2)}, u32[]{:S(2)}) collective-permute-start(s32[384]{0:T(512)} %param.23), channel_id=1, source_target_pairs={{0,4},{4,8},{8,12},{12,16},{16,20},{20,24},{24,28},{1,5},{5,9},{9,... | collective-permute-start | bytes 4616 | tf_op jit(solution)/shard_map/ppermute | solution.py:21
  26.6 20.5 %collective-permute-start = (bf16[384,512]{1,0:T(8,128)(2,1)S(1)}, bf16[384,512]{1,0:T(8,128)(2,1)S(1)}, u32[]{:S(2)}, u32[]{:S(2)}) collective-permute-start(bf16[384,512]{1,0:T(8,128)(2,1)S(1)} %copy-done.5), channel_id=1, source_target_pairs={{0,12},{4,16},{8,20},{12,24},{16,28},{1,13},{5,17},{9,21},{13,25},... | collective-permute-start | bytes 1179656 | tf_op jit(solution)/shard_map/ppermute | solution.py:21
  29.2 32.3 %collective-permute-start.1 = (bf16[384,512]{1,0:T(8,128)(2,1)S(1)}, bf16[384,512]{1,0:T(8,128)(2,1)S(1)}, u32[]{:S(2)}, u32[]{:S(2)}) collective-permute-start(bf16[384,512]{1,0:T(8,128)(2,1)S(1)} %copy-done.5), channel_id=1, source_target_pairs={{0,8},{4,12},{8,16},{12,20},{16,24},{20,28},{1,9},{5,13},{9,17},{1... | collective-permute-start | bytes 1179656 | tf_op jit(solution)/shard_map/ppermute | solution.py:21
  30.5 31.0 %collective-permute-start.2 = (bf16[384,512]{1,0:T(8,128)(2,1)S(1)}, bf16[384,512]{1,0:T(8,128)(2,1)S(1)}, u32[]{:S(2)}, u32[]{:S(2)}) collective-permute-start(bf16[384,512]{1,0:T(8,128)(2,1)S(1)} %copy-done.5), channel_id=1, source_target_pairs={{0,4},{4,8},{8,12},{12,16},{16,20},{20,24},{24,28},{1,5},{5,9},{9,... | collective-permute-start | bytes 1179656 | tf_op jit(solution)/shard_map/ppermute | solution.py:21
  47.1 28.3 %collective-permute-start.8 = (bf16[384,64]{0,1:T(8,128)(2,1)S(1)}, bf16[384,64]{0,1:T(8,128)(2,1)S(1)}, u32[]{:S(2)}, u32[]{:S(2)}) collective-permute-start(bf16[384,64]{0,1:T(8,128)(2,1)S(1)} %pad_maximum_fusion.4), channel_id=1, source_target_pairs={{0,4},{4,8},{8,12},{12,16},{16,20},{20,24},{24,28},{1,5},{5,9},{9,... | collective-permute-start | bytes 147464 | tf_op jit(solution)/shard_map/ppermute | solution.py:21
  63.5 8.3 %copy-start.17 = (bf16[512,1024]{1,0:T(8,128)(2,1)S(1)}, bf16[512,1024]{1,0:T(8,128)(2,1)}, u32[]{:S(2)}) copy-start(bf16[512,1024]{1,0:T(8,128)(2,1)} %param.25) | copy-start | bytes 3145732
  125.9 16.3 %copy-start.10 = (bf16[512]{0:T(512)(128)(2,1)S(1)}, bf16[512]{0:T(512)(128)(2,1)}, u32[]{:S(2)}) copy-start(bf16[512]{0:T(512)(128)(2,1)} %param.27) | copy-start | bytes 3076
  125.9 16.3 %copy-start.11 = (bf16[512]{0:T(512)(128)(2,1)S(1)}, bf16[512]{0:T(512)(128)(2,1)}, u32[]{:S(2)}) copy-start(bf16[512]{0:T(512)(128)(2,1)} %param.28) | copy-start | bytes 3076
  125.9 16.3 %copy-start.8 = (bf16[3,1408]{1,0:T(4,128)(2,1)S(1)}, bf16[3,1408]{1,0:T(4,128)(2,1)}, u32[]{:S(2)}) copy-start(bf16[3,1408]{1,0:T(4,128)(2,1)} %param.31) | copy-start | bytes 25348
  125.9 16.3 %copy-start.9 = (bf16[3,1408]{1,0:T(4,128)(2,1)S(1)}, bf16[3,1408]{1,0:T(4,128)(2,1)}, u32[]{:S(2)}) copy-start(bf16[3,1408]{1,0:T(4,128)(2,1)} %param.32) | copy-start | bytes 25348
  125.9 24.0 %copy-start.3 = (bf16[384,512]{1,0:T(8,128)(2,1)S(1)}, bf16[384,512]{1,0:T(8,128)(2,1)}, u32[]{:S(2)}) copy-start(bf16[384,512]{1,0:T(8,128)(2,1)} %param.18) | copy-start | bytes 1179652
  125.9 23.7 %all-to-all-start = ((bf16[4,384,512]{2,1,0:T(8,128)(2,1)}), bf16[4,384,512]{2,1,0:T(8,128)(2,1)S(1)}, u32[]{:S(2)}, u32[]{:S(2)}) async-start(bf16[4,384,512]{2,1,0:T(8,128)(2,1)} %pad_maximum_fusion), calls=%async_computation | async-start | bytes 3145728 | tf_op jit(solution)/shard_map/all_to_all | solution.py:47
  129.7 13.7 %collective-permute-start.10 = (s32[2]{0:T(128)S(1)}, s32[2]{0:T(128)S(1)}, u32[]{:S(2)}, u32[]{:S(2)}) collective-permute-start(s32[2]{0:T(128)S(1)} %slice.108), channel_id=1, source_target_pairs={{0,4},{4,8},{8,12},{12,16},{16,20},{20,24},{24,28},{1,5},{5,9},{9,... | collective-permute-start | bytes 32 | tf_op jit(solution)/shard_map/ppermute | solution.py:21
  156.4 17.2 %copy-start.2 = (bf16[384,512]{1,0:T(8,128)(2,1)}, bf16[384,512]{1,0:T(8,128)(2,1)S(1)}, u32[]{:S(2)}) copy-start(bf16[384,512]{1,0:T(8,128)(2,1)S(1)} %add_convert_fusion.1) | copy-start | bytes 1179652
  180.0 144.1 %collective-permute-start.11 = (bf16[2,1408]{1,0:T(2,128)(2,1)S(1)}, bf16[2,1408]{1,0:T(2,128)(2,1)S(1)}, u32[]{:S(2)}, u32[]{:S(2)}) collective-permute-start(bf16[2,1408]{1,0:T(2,128)(2,1)S(1)} %slice.137), channel_id=1, source_target_pairs={{0,4},{4,8},{8,12},{12,16},{16,20},{20,24},{24,28},{1,5},{5,9},{9,... | collective-permute-start | bytes 16904 | tf_op jit(solution)/shard_map/ppermute | solution.py:21
  228.1 96.0 %collective-permute-start.9 = (bf16[2,1408]{1,0:T(2,128)(2,1)S(1)}, bf16[2,1408]{1,0:T(2,128)(2,1)S(1)}, u32[]{:S(2)}, u32[]{:S(2)}) collective-permute-start(bf16[2,1408]{1,0:T(2,128)(2,1)S(1)} %slice.134), channel_id=1, source_target_pairs={{0,4},{4,8},{8,12},{12,16},{16,20},{20,24},{24,28},{1,5},{5,9},{9,... | collective-permute-start | bytes 16904 | tf_op jit(solution)/shard_map/ppermute | solution.py:21
  315.7 8.4 %copy-start.15 = (bf16[384,1408]{1,0:T(8,128)(2,1)S(1)}, bf16[384,1408]{1,0:T(8,128)(2,1)}, u32[]{:S(2)}) copy-start(bf16[384,1408]{1,0:T(8,128)(2,1)} %copy-done.14) | copy-start | bytes 3244036
  335.0 3.7 copy-start.12
  335.0 3.7 copy-start.13
  335.0 23.7 %all-to-all-start.1 = ((bf16[4,384,512]{2,1,0:T(8,128)(2,1)}), bf16[4,384,512]{2,1,0:T(8,128)(2,1)S(1)}, u32[]{:S(2)}, u32[]{:S(2)}) async-start(bf16[4,384,512]{2,1,0:T(8,128)(2,1)} %pad_maximum_fusion.1), calls=%async_computation.1 | async-start | bytes 3145728 | tf_op jit(solution)/shard_map/all_to_all | solution.py:47
  338.7 29.2 %copy-start.1 = (bf16[512,1024]{1,0:T(8,128)(2,1)S(1)}, bf16[512,1024]{1,0:T(8,128)(2,1)}, u32[]{:S(2)}) copy-start(bf16[512,1024]{1,0:T(8,128)(2,1)} %param.24) | copy-start | bytes 3145732
  (3 other events, 5.5 us)
Sparse Core Ops, SparseCore 0:
  9.5 118.1 all-gather.6
  129.9 92.8 all-gather.4
  225.0 90.6 all-gather.8
